TPU v7x, 32 devices: a whole 2x2x4 slice. The times are simulated.
32 devices in a mesh: rep: 2 (over y), fs: 4 (over z), tp: 4 (over x, core).
Axes of the slice: x: 2, y: 2, z: 4, core: 2. Of those that a mesh axis runs over, the one named last changes fastest.
Arguments:
- tokens: bfloat16 [4096, 2048], P(('rep', 'fs')), may hold values from -6 to 6
- norm_gain: float32 [2048], replicated, may hold values from 0.1 to 1.9
- gate_weight: bfloat16 [2048, 5632], P('fs', 'tp'), may hold values from -0.125 to 0.125
- up_weight: bfloat16 [2048, 5632], P('fs', 'tp'), may hold values from -0.125 to 0.125
- down_weight: bfloat16 [5632, 2048], P('tp', 'fs'), may hold values from -0.078125 to 0.078125
Outputs:
- branch_out: bfloat16 [4096, 2048], P(('rep', 'fs'))
All inputs are finite; a program needn't handle non-finite values.
Results may differ from a plain program's by a relative error of at most 0.014.
Values may be sent and summed in bfloat16 or wider, within the bound.
A program may use at most 64 MiB of HBM per device.

v0:
```python
import functools

import jax
import jax.numpy as jnp
from jax import lax
from jax.experimental import pallas as pl
from jax.experimental.pallas import tpu as pltpu
from jax.sharding import PartitionSpec as P

MESH = pl.DeviceIdType.MESH
F32 = jnp.float32
BF16 = jnp.bfloat16


def plain(tokens, norm_gain, gate_weight, up_weight, down_weight):
    wide_tok = tokens.astype(F32)
    scale = lax.rsqrt(jnp.mean(wide_tok * wide_tok, axis=-1, keepdims=True) + 1e-06)
    normed = (wide_tok * scale * norm_gain).astype(BF16)
    gate = jnp.dot(normed, lax.all_gather(gate_weight, "fs", axis=0, tiled=True), preferred_element_type=F32)
    up = jnp.dot(normed, lax.all_gather(up_weight, "fs", axis=0, tiled=True), preferred_element_type=F32)
    hidden = (jax.nn.silu(gate) * up).astype(BF16)
    down = lax.all_gather(down_weight, "fs", axis=1, tiled=True)
    partial_value = jnp.dot(hidden, down, preferred_element_type=F32)
    return lax.psum(partial_value.astype(BF16), "tp")


CHUNKS = 2
LAG = 2


def kernel(
    n, tok_ref, gain_ref, wg_ref, wu_ref, wd_ref, out_ref,
    tokp, normed, bg, bu, bd, gate, up, hidden, part, r1, sbuf, rz, sx, r2, outv,
    loc_sem, zsend, zrecv, ysend, yrecv, tsend, trecv,
    psend, precv, wsend, wrecv, xsend, xrecv, qsend, qrecv, osem,
):
    z = lax.axis_index("fs")
    y = lax.axis_index("rep")
    t = lax.axis_index("tp")
    c = lax.rem(t, 2)
    tokens, width = tok_ref.shape
    depth, units = wg_ref.shape
    cols = wd_ref.shape[1] // CHUNKS
    half_k, half_t, quarter = depth // 2, tokens // 2, tokens // 4
    mid = 128
    most = (units - mid) // 2
    e = lax.rem(z, 2)
    low = z - e
    pair = {"fs": z + 1 - 2 * e}
    has_mid = e == c
    parts = ((0, most, 0), (most, mid, c), (most + mid, most, 1))
    mine = pl.multiple_of(e * (most + mid), mid)
    spans = ((mine, most), (most, mid))
    mate = {"tp": t + 1 - 2 * c}
    across = {"tp": lax.rem(t + 2, 4)}
    peer = {"rep": 1 - y}

    barrier = pltpu.get_barrier_semaphore()

    around = ({"fs": lax.rem(z + 1, n)}, {"fs": lax.rem(z + n - 1, n)})
    others = tuple({"tp": lax.rem(t + d, 4)} for d in (1, 2, 3))
    for one in around + others + (peer,):
        pl.semaphore_signal(barrier, 1, device_id=one, device_id_type=MESH)
    pl.semaphore_wait(barrier, 6)

    def token_move(quart, to, sem, first):
        at = pl.ds(pl.multiple_of(quart * quarter, quarter), quarter)
        return pltpu.make_async_remote_copy(
            src_ref=(tok_ref if first else tokp).at[at],
            dst_ref=tokp.at[at],
            send_sem=tsend.at[sem],
            recv_sem=trecv.at[quart],
            device_id=to,
            device_id_type=MESH,
        )

    token_move(t, pair, 0, True).start()

    def window(u, span, who):
        start, size = span
        if u < 2:
            return (pl.ds(pl.multiple_of(who * half_k, half_k), half_k), pl.ds(start, size))
        row = start + who * (size // 2)
        return (pl.ds(pl.multiple_of(row, 64), size // 2),)

    def slot(u, blk, span, who):
        if u < 2:
            return (bg, bu)[u].at[(blk,) + window(u, span, who)]
        return bd.at[(blk, u - 2) + window(u, span, who)]

    def own(u, span):
        if u < 2:
            return (wg_ref, wu_ref)[u].at[window(u, span, y)]
        return wd_ref.at[window(u, span, y) + (pl.ds((u - 2) * cols, cols),)]

    def along(u, blk, p, way, first=False):
        span = parts[p][:2]
        return pltpu.make_async_remote_copy(
            src_ref=own(u, span) if first else slot(u, blk, span, y),
            dst_ref=slot(u, blk, span, y),
            send_sem=zsend.at[u, blk, p, way],
            recv_sem=zrecv.at[u, blk, p],
            device_id={"fs": z - 1 + 2 * way},
            device_id_type=MESH,
        )

    def passes(p, way):
        q = parts[p][2]
        return jnp.logical_or(
            jnp.logical_and(way == 0, z > q), jnp.logical_and(way == 1, z < n - 2 + q))

    def arrives(p, way):
        q = parts[p][2]
        return jnp.logical_or(
            jnp.logical_and(way == 0, z >= q), jnp.logical_and(way == 1, z < n - 1 + q))

    def swap(u, blk, i, who):
        return pltpu.make_async_remote_copy(
            src_ref=slot(u, blk, spans[i], who),
            dst_ref=slot(u, blk, spans[i], who),
            send_sem=ysend.at[u, blk, i],
            recv_sem=yrecv.at[u, blk, i],
            device_id=peer,
            device_id_type=MESH,
        )

    def send_own(units_now, way):
        for u in units_now:
            for p in range(3):
                pl.when(passes(p, jnp.int32(way)))(lambda: along(u, z, p, way, True).start())

    D_UNITS = tuple(range(2, 2 + CHUNKS))
    send_own((0, 1), 0)
    send_own((0, 1), 1)
    pl.when(z == n - 1)(lambda: send_own(D_UNITS, 0))
    pl.when(z == 0)(lambda: send_own(D_UNITS, 1))

    locals_ = [
        pltpu.make_async_copy(wg_ref, bg.at[z], loc_sem.at[0]),
        pltpu.make_async_copy(wu_ref, bu.at[z], loc_sem.at[1]),
    ] + [
        pltpu.make_async_copy(wd_ref.at[:, pl.ds(j * cols, cols)], bd.at[z, j], loc_sem.at[2 + j])
        for j in range(CHUNKS)
    ]
    for copy in locals_:
        copy.start()

    step = 64

    def norm(src, base):
        @pl.loop(0, tokens // step)
        def _(i):
            at = pl.ds(pl.multiple_of(i * step, step), step)
            to = pl.ds(pl.multiple_of(base + i * step, step), step)
            wide = src[at, :].astype(F32)
            scale = lax.rsqrt(jnp.mean(wide * wide, axis=-1, keepdims=True) + 1e-06)
            normed[to, :] = (wide * scale * gain_ref[...]).astype(BF16)

    norm(tok_ref, 0)

    def add_dot(u, blk, first=False):
        total, held = (gate, bg) if u == 0 else (up, bu)

        def piece(start, size, base):
            @pl.loop(0, 4)
            def _(i):
                at = pl.ds(pl.multiple_of(i * half_t, half_t), half_t)
                left = normed[at, pl.ds(pl.multiple_of(blk * depth, depth), depth)]
                value = jnp.dot(left, held[blk, :, pl.ds(start, size)], preferred_element_type=F32)
                to = pl.ds(base, size)
                total[at, to] = value if first else total[at, to] + value

        piece(mine, most, 0)
        pl.when(has_mid)(lambda: piece(most, mid, most))

    def place(blk, j, who):
        return (
            pl.ds(pl.multiple_of(who * half_t, half_t), half_t),
            pl.ds(pl.multiple_of(blk * (cols * CHUNKS) + j * cols, cols), cols),
        )

    def to_mate(blk, j):
        return pltpu.make_async_remote_copy(
            part.at[blk, j, 1], r1.at[blk, j], psend.at[blk, j], precv.at[blk, j],
            device_id=mate, device_id_type=MESH)

    def to_across(blk, j):
        return pltpu.make_async_remote_copy(
            sx.at[blk, j], r2.at[blk, j], xsend.at[blk, j], xrecv.at[blk, j],
            device_id=across, device_id_type=MESH)

    def give(blk, j, who):
        return pltpu.make_async_remote_copy(
            outv.at[place(blk, j, who)], outv.at[place(blk, j, who)], qsend.at[blk, j], qrecv.at[blk, j],
            device_id=mate, device_id_type=MESH)

    def write(blk, j):
        at = pl.ds(pl.multiple_of(blk * (cols * CHUNKS) + j * cols, cols), cols)
        return pltpu.make_async_copy(outv.at[:, at], out_ref.at[:, at], osem.at[blk, j])

    def to_pair(blk, j):
        return pltpu.make_async_remote_copy(
            sbuf.at[blk, j, 1], rz.at[blk, j], wsend.at[blk, j], wrecv.at[blk, j],
            device_id=pair, device_id_type=MESH)

    def make_part(blk, j):
        def fill(with_mid):
            @pl.loop(0, 4)
            def _(i):
                side, which = i // 2, lax.rem(i, 2)
                whose = c + side - 2 * c * side
                at = pl.ds(pl.multiple_of(which * tokens + whose * half_t, half_t), half_t)
                value = jnp.dot(
                    hidden[at, pl.ds(0, most)], bd[blk, j, pl.ds(mine, most), :], preferred_element_type=F32)
                if with_mid:
                    value = value + jnp.dot(
                        hidden[at, pl.ds(most, mid)], bd[blk, j, pl.ds(most, mid), :], preferred_element_type=F32)
                part[blk, j, side, which] = value.astype(BF16)

        pl.when(has_mid)(lambda: fill(True))
        pl.when(jnp.logical_not(has_mid))(lambda: fill(False))
        to_mate(blk, j).start()

    def add_pair(blk, j):
        to_mate(blk, j).wait_recv()
        sbuf[blk, j] = (part[blk, j, 0].astype(F32) + r1[blk, j].astype(F32)).astype(BF16)
        to_pair(blk, j).start()

    def add_line(blk, j):
        to_pair(blk, j).wait_recv()
        sx[blk, j] = (sbuf[blk, j, 0].astype(F32) + rz[blk, j].astype(F32)).astype(BF16)
        to_across(blk, j).start()

    def finish(blk, j):
        to_across(blk, j).wait_recv()
        outv[place(blk, j, c)] = (sx[blk, j].astype(F32) + r2[blk, j].astype(F32)).astype(BF16)
        give(blk, j, c).start()

    def store(blk, j):
        give(blk, j, 1 - c).wait_recv()
        write(blk, j).start()

    def sides(k, body):
        @pl.loop(0, 2)
        def _(way):
            blk = z + k - 2 * k * way

            @pl.when(jnp.logical_and(blk >= 0, blk < n))
            def _():
                body(blk, way)

    def forward(u, k):
        def body(blk, way):
            for p in range(3):
                @pl.when(arrives(p, way))
                def _():
                    along(u, blk, p, way).wait_recv()
                    pl.when(passes(p, way))(lambda: along(u, blk, p, way).start())

            swap(u, blk, 0, y).start()
            pl.when(has_mid)(lambda: swap(u, blk, 1, y).start())

        sides(k, body)

    def use(u, k):
        def body(blk, way):
            swap(u, blk, 0, 1 - y).wait_recv()
            pl.when(has_mid)(lambda: swap(u, blk, 1, 1 - y).wait_recv())
            if u < 2:
                add_dot(u, blk)
            else:
                make_part(blk, u - 2)

        sides(k, body)
        if u >= 2:
            advance(k, u - 2)

    def reached(k, body):
        @pl.loop(0, 2)
        def _(way):
            blk = low + k + (1 - 2 * k) * way
            pl.when(jnp.logical_and(blk >= 0, blk < n))(lambda: body(blk))

    summed, crossing, closing = [], [], []

    def drain():
        if closing:
            k, j = closing.pop()
            reached(k, lambda blk: store(blk, j))
        if crossing:
            k, j = crossing.pop()
            reached(k, lambda blk: finish(blk, j))
            closing.append((k, j))
        if summed:
            k, j = summed.pop()
            reached(k, lambda blk: add_line(blk, j))
            crossing.append((k, j))

    def advance(k, j):
        drain()
        run(k, lambda blk: add_pair(blk, j))
        if k > 0:
            summed.append((k, j))

    def run(k, body):
        if k == 0:
            body(z)
        else:
            sides(k, lambda blk, way: body(blk))

    def middle():
        @pl.loop(0, 2 * tokens // step)
        def _(i):
            at = pl.ds(pl.multiple_of(i * step, step), step)
            value = gate[at, :]
            hidden[at, :] = (value / (1.0 + jnp.exp(-value)) * up[at, :]).astype(BF16)

        for j in range(CHUNKS):
            locals_[2 + j].wait()
            make_part(z, j)
            advance(0, j)

    token_move(t, pair, 0, True).wait_recv()
    for i, one in enumerate(others):
        token_move(t, one, 1 + i, False).start()

    def prepare():
        for d in (1, 2, 3):
            token_move(lax.rem(t + d, 4), mate, 0, False).wait_recv()
        norm(tokp, tokens)
        for u in (0, 1):
            locals_[u].wait()
            add_dot(u, z, first=True)

    events = [(u, k) for k in range(1, n) for u in (0, 1)]
    last_row = len(events)
    events += [(u, k) for k in range(1, n) for u in D_UNITS]
    for i in range(len(events) + LAG):
        if i < len(events):
            u, k = events[i]
            forward(u, k)
            if u == 1:
                pl.when(jnp.logical_and(n - 1 - z == k, z > 0))(lambda: send_own(D_UNITS, 0))
                pl.when(jnp.logical_and(z == k, z < n - 1))(lambda: send_own(D_UNITS, 1))
        if i == 0:
            prepare()
        if i >= LAG:
            use(*events[i - LAG])
            if i - LAG == last_row - 1:
                middle()
    for _ in range(3):
        drain()

    token_move(t, pair, 0, True).wait_send()
    for i, one in enumerate(others):
        token_move(t, one, 1 + i, False).wait_send()
    for u in range(2 + CHUNKS):
        for p in range(3):
            for way in (0, 1):
                pl.when(passes(p, jnp.int32(way)))(lambda: along(u, z, p, way, True).wait_send())
        for k in range(1, n):
            def sent(blk, way):
                for p in range(3):
                    pl.when(jnp.logical_and(arrives(p, way), passes(p, way)))(
                        lambda: along(u, blk, p, way).wait_send())
                swap(u, blk, 0, y).wait_send()
                pl.when(has_mid)(lambda: swap(u, blk, 1, y).wait_send())

            sides(k, sent)

    @pl.loop(0, n)
    def _(blk):
        for j in range(CHUNKS):
            to_mate(blk, j).wait_send()
            to_pair(blk, j).wait_send()
            to_across(blk, j).wait_send()
            give(blk, j, c).wait_send()
            write(blk, j).wait()


def fused(n, tokens, norm_gain, gate_weight, up_weight, down_weight):
    rows, width = tokens.shape
    depth, units = gate_weight.shape
    cols = down_weight.shape[1] // CHUNKS
    held = (units + 128) // 2
    dma = pltpu.SemaphoreType.DMA
    grid_of = (n, CHUNKS)
    hbm = pl.BlockSpec(memory_space=pl.ANY)
    vmem = pl.BlockSpec(memory_space=pltpu.VMEM)
    return pl.pallas_call(
        functools.partial(kernel, n),
        out_shape=jax.ShapeDtypeStruct((rows, width), BF16),
        in_specs=[vmem, vmem, hbm, hbm, hbm],
        out_specs=hbm,
        scratch_shapes=[
            pltpu.VMEM((rows, width), BF16),
            pltpu.VMEM((2 * rows, width), BF16),
            pltpu.VMEM((n, depth, units), BF16),
            pltpu.VMEM((n, depth, units), BF16),
            pltpu.VMEM((n, CHUNKS, units, cols), BF16),
            pltpu.VMEM((2 * rows, held), F32),
            pltpu.VMEM((2 * rows, held), F32),
            pltpu.VMEM((2 * rows, held), BF16),
            pltpu.VMEM((n, CHUNKS, 2, 2, rows // 2, cols), BF16),
            pltpu.VMEM((n, CHUNKS, 2, rows // 2, cols), BF16),
            pltpu.VMEM((n, CHUNKS, 2, rows // 2, cols), BF16),
            pltpu.VMEM((n, CHUNKS, rows // 2, cols), BF16),
            pltpu.VMEM((n, CHUNKS, rows // 2, cols), BF16),
            pltpu.VMEM((n, CHUNKS, rows // 2, cols), BF16),
            pltpu.VMEM((rows, width), BF16),
            dma((2 + CHUNKS,)),
            dma((2 + CHUNKS, n, 3, 2)),
            dma((2 + CHUNKS, n, 3)),
            dma((2 + CHUNKS, n, 2)),
            dma((2 + CHUNKS, n, 2)),
            dma((4,)),
            dma((4,)),
        ] + [dma(grid_of) for _ in range(9)],
        compiler_params=pltpu.CompilerParams(
            collective_id=0, has_side_effects=True, vmem_limit_bytes=60 * 2**20
        ),
    )(tokens, norm_gain.reshape(1, width), gate_weight, up_weight, down_weight)


def solution(mesh):
    n = mesh.shape["fs"]
    small = mesh.shape["rep"] == 2 and mesh.shape["tp"] == 4 and n == 4
    body = functools.partial(fused, n) if small else plain
    in_specs = (P(("rep", "fs"), None), P(), P("fs", "tp"), P("fs", "tp"), P("tp", "fs"))
    out_specs = P(("rep", "fs"), None)
    return jax.shard_map(
        body, mesh=mesh, in_specs=in_specs, out_specs=out_specs, check_vma=False
    )
```

profile of v0, /device:TPU:1, one launch (start us, length us, event | category | flops | bytes accessed | tf_op | source)
XLA Modules:
  0.0 146.7 jit_solution(17595181846958895348)
XLA Ops:
  0.0 143.6 %shard_map.55 = bf16[512,2048]{1,0:T(8,128)(2,1)} custom-call(bf16[512,2048]{1,0:T(8,128)(2,1)} %tok_ref.1, f32[1,2048]{1,0:T(1,128)} %bitcast.1, bf16[512,1408]{1,0:T(8,128)(2,1)} %wg_ref.1, bf16[512,1408]{1,0:T(8,128)(2,1)} %wu_ref.1, bf16[1408,512]{1,0:T(8,128)(2,1)} %wd_ref.1), custom_call_target="tpu_custom_call" | custom-call | tf_op jit(solution)/shard_map/pallas_call | solution.py:390
  143.6 3.2 %copy.7 = bf16[512,2048]{1,0:T(8,128)(2,1)} copy(bf16[512,2048]{1,0:T(8,128)(2,1)} %shard_map.55) | data formatting | bytes 4194304
where the time goes:
time: 147 us
  Pallas kernels  144 us (98%)
  local copies, waits for them, and re-layouts  3.16 us (2%)
    pallas_call x1, Pallas kernels, fused(): pl.pallas_call(functools.partial(kernel, n), out_shape=jax.ShapeDtypeStru...  144 us
    unnamed x1, local copies, waits for them, and re-layouts  3.16 us

commit v1 on v0

v1 whole, which is shorter than its diff:
```python
import functools

import jax
import jax.numpy as jnp
from jax import lax
from jax.experimental import pallas as pl
from jax.experimental.pallas import tpu as pltpu
from jax.sharding import PartitionSpec as P

MESH = pl.DeviceIdType.MESH
F32 = jnp.float32
BF16 = jnp.bfloat16


def plain(tokens, norm_gain, gate_weight, up_weight, down_weight):
    wide_tok = tokens.astype(F32)
    scale = lax.rsqrt(jnp.mean(wide_tok * wide_tok, axis=-1, keepdims=True) + 1e-06)
    normed = (wide_tok * scale * norm_gain).astype(BF16)
    gate = jnp.dot(normed, lax.all_gather(gate_weight, "fs", axis=0, tiled=True), preferred_element_type=F32)
    up = jnp.dot(normed, lax.all_gather(up_weight, "fs", axis=0, tiled=True), preferred_element_type=F32)
    hidden = (jax.nn.silu(gate) * up).astype(BF16)
    down = lax.all_gather(down_weight, "fs", axis=1, tiled=True)
    partial_value = jnp.dot(hidden, down, preferred_element_type=F32)
    return lax.psum(partial_value.astype(BF16), "tp")


CUTS = ((2, 2), (2, 1, 1))
KINDS = (1, 0, 0, 1)
MOST_CUTS = 3
SUBS = 2
MID = 128


def spans_of(which, width):
    spans, at = [], 0
    for part in CUTS[which]:
        spans.append((at, part * width // 4))
        at += part * width // 4
    return spans


def plan(width):
    block, hop, start = 15.4, 2.2, 67.2
    free = {"x": 0.0, "z": 0.0, "weights": 71.7, "core": 74.0}
    todo = [(72.0, "last", 0, 0)]

    def book(link, when, size):
        free[link] = max(free[link], when) + size
        return free[link]

    for s in range(4):
        for i, (at, size) in enumerate(spans_of(KINDS[s], width)):
            share = block * size / width
            ready = 70.0
            if s == 1:
                out = 64.0 + block * (at + size) / width / 2 + hop
                todo.append((out, "end", s, i))
                ready = out + share / 2 + hop
            if s >= 2:
                begin = start + (s - 2) * block + block * at / width
                far, near = begin + 0.55 * share + hop, begin + share + hop
                out = book("weights", far, share / 2) + hop
                todo += [(far, "far", s, i), (near, "near", s, i), (out, "end", s, i)]
                ready = max(near, out) + share / 2 + hop
            done = book("core", ready, 1.2 * size / 256 + 0.2)
            todo.append((done, "use", s, i))
    uses = [(when, s, i) for when, kind, s, i in todo if kind == "use"]
    pend = [(when + 1.8, 1, s, i) for when, s, i in uses]
    while pend:
        pend.sort()
        when, stage, s, i = pend.pop(0)
        todo.append((when, stage, s, i))
        size = spans_of(KINDS[s], width)[i][1]
        half = block * size / width * 5.5 / 15.4
        path = ROUTES[direct(s, i)]
        if stage <= len(path):
            link, scale = path[stage - 1]
            after = when + 1.5 if link == "core" else book(link, when, half * scale) + hop
            pend.append((after, stage + 1, s, i))
    todo.sort(key=lambda item: item[0])
    return [item[1:] for item in todo]


ROUTES = (
    (("x", 1.0), ("z", 0.8), ("x", 0.5), ("core", 0.0)),
    (("z", 1.0), ("x", 1.0), ("core", 0.0)),
)


def direct(s, i):
    return int(s == 3 or s == 1)


def kernel(
    n, tok_ref, gain_ref, wg_ref, wu_ref, wd_ref, out_ref,
    tokv, tokp, normed, bw, bd, acc, hidden, part, r1, sbuf, rz, sx, r2, outv,
    loc_sem, zsend, zrecv, dsend, drecv, ysend, yrecv, vsend, vrecv, tsend, trecv,
    psend, precv, wsend, wrecv, xsend, xrecv, asend, arecv, qsend, qrecv, osem,
):
    z = lax.axis_index("fs")
    y = lax.axis_index("rep")
    t = lax.axis_index("tp")
    c = lax.rem(t, 2)
    tokens, width = tok_ref.shape
    depth, units = wg_ref.shape
    cols = wd_ref.shape[1]
    spans = tuple(spans_of(which, cols) for which in (0, 1))
    half_k, half_t, quarter = depth // 2, tokens // 2, tokens // 4
    sub_k = half_k // SUBS
    most = (units - MID) // 2
    e = lax.rem(z, 2)
    hi = z // 2
    inner = e != hi
    near = z + 1 - 2 * e
    third = 2 - hi
    fourth = 3 - 3 * hi
    pair = {"fs": near}
    has_mid = e == c
    mine = pl.multiple_of(e * (most + MID), MID)
    first_unit = pl.multiple_of(e * jnp.where(has_mid, most, most + MID), MID)
    mate = {"tp": t + 1 - 2 * c}
    across = {"tp": lax.rem(t + 2, 4)}
    row = t // 2
    first_block, second_block = 3 * hi, 1 + hi
    peer = {"rep": 1 - y}

    barrier = pltpu.get_barrier_semaphore()

    around = ({"fs": lax.rem(z + 1, n)}, {"fs": lax.rem(z + n - 1, n)})
    others = tuple({"tp": lax.rem(t + d, 4)} for d in (1, 2, 3))
    for one in around + others + (peer,):
        pl.semaphore_signal(barrier, 1, device_id=one, device_id_type=MESH)
    tok_copy = pltpu.make_async_copy(tok_ref, tokv, loc_sem.at[3])
    tok_copy.start()
    pl.semaphore_wait(barrier, 6)

    def token_move(quart, to, sem, first):
        at = pl.ds(pl.multiple_of(quart * quarter, quarter), quarter)
        return pltpu.make_async_remote_copy(
            src_ref=(tok_ref if first else tokp).at[at],
            dst_ref=tokp.at[at],
            send_sem=tsend.at[sem],
            recv_sem=trecv.at[quart],
            device_id=to,
            device_id_type=MESH,
        )

    def start_of(r, way):
        if r == 1:
            return most, MID
        side = way if r == 0 else 1 - way
        return pl.multiple_of(side * (most + MID), MID), most

    def side_of(r, way):
        return c if r == 1 else (way if r == 0 else 1 - way)

    def passes(r, way):
        q = side_of(r, way)
        return jnp.logical_or(
            jnp.logical_and(way == 0, z > q), jnp.logical_and(way == 1, z < n - 2 + q))

    def arrives(r, way):
        q = side_of(r, way)
        return jnp.logical_or(
            jnp.logical_and(way == 0, z >= q), jnp.logical_and(way == 1, z < n - 1 + q))

    def pieces(r):
        return range(1 if r == 1 else SUBS)

    def rows_of(r, s, who):
        if r == 1:
            return pl.ds(pl.multiple_of(who * half_k, half_k), half_k)
        return pl.ds(pl.multiple_of(who * half_k + s * sub_k, sub_k), sub_k)

    def along(u, blk, r, s, way, own=None):
        start, size = start_of(r, way)
        at = (rows_of(r, s, y), pl.ds(start, size))
        return pltpu.make_async_remote_copy(
            src_ref=bw.at[(u, blk) + at] if own is None else own.at[at],
            dst_ref=bw.at[(u, blk) + at],
            send_sem=zsend.at[u, blk, r, s, way],
            recv_sem=zrecv.at[u, blk, r, s],
            device_id={"fs": z - 1 + 2 * way},
            device_id_type=MESH,
        )

    def swap(u, blk, i, s, who):
        start, size = ((mine, most), (most, MID))[i]
        place = bw.at[u, blk, rows_of(i, s, who), pl.ds(start, size)]
        return pltpu.make_async_remote_copy(
            src_ref=place,
            dst_ref=place,
            send_sem=ysend.at[u, blk, i, s],
            recv_sem=yrecv.at[u, blk, i, s],
            device_id=peer,
            device_id_type=MESH,
        )

    def d_rows(start, size, who):
        return pl.ds(pl.multiple_of(start + who * (size // 2), 64), size // 2)

    def d_along(blk, i, span, r, way, own=False):
        start, size = start_of(r, way)
        at = (d_rows(start, size, y), pl.ds(*span))
        return pltpu.make_async_remote_copy(
            src_ref=wd_ref.at[at] if own else bd.at[(blk,) + at],
            dst_ref=bd.at[(blk,) + at],
            send_sem=dsend.at[blk, i, r, way],
            recv_sem=drecv.at[blk, i, r],
            device_id={"fs": z - 1 + 2 * way},
            device_id_type=MESH,
        )

    def d_swap(blk, i, span, p, who):
        start, size = ((mine, most), (most, MID))[p]
        place = bd.at[blk, d_rows(start, size, who), pl.ds(*span)]
        return pltpu.make_async_remote_copy(
            src_ref=place,
            dst_ref=place,
            send_sem=vsend.at[blk, i, p],
            recv_sem=vrecv.at[blk, i, p],
            device_id=peer,
            device_id_type=MESH,
        )

    def own_pieces(way, body):
        for u, own in ((0, wg_ref), (1, wu_ref)):
            for r in range(3):
                @pl.when(passes(r, way))
                def _():
                    for s in pieces(r):
                        body(along(u, z, r, s, way, own))

    def own_d_pieces(which, way, body):
        for i, span in enumerate(spans[which]):
            for r in range(3):
                pl.when(passes(r, way))(lambda: body(d_along(z, i, span, r, way, True)))

    go = lambda copy: copy.start()
    ZERO, ONE = jnp.int32(0), jnp.int32(1)
    inward, outward = 1 - hi, hi
    @pl.when(inner)
    def _():
        own_pieces(inward, go)
        token_move(t, pair, 0, True).start()
        own_pieces(outward, go)

    @pl.when(jnp.logical_not(inner))
    def _():
        token_move(t, pair, 0, True).start()
        own_pieces(inward, go)
        own_d_pieces(1, inward, go)

    locals_ = [
        pltpu.make_async_copy(wg_ref, bw.at[0, z], loc_sem.at[0]),
        pltpu.make_async_copy(wu_ref, bw.at[1, z], loc_sem.at[1]),
        pltpu.make_async_copy(wd_ref, bd.at[z], loc_sem.at[2]),
    ]
    for copy in locals_:
        copy.start()

    step = 64

    def norm(src, base):
        @pl.loop(0, tokens // step)
        def _(i):
            at = pl.ds(pl.multiple_of(i * step, step), step)
            to = pl.ds(pl.multiple_of(base + i * step, step), step)
            wide = src[at, :].astype(F32)
            scale = lax.rsqrt(jnp.mean(wide * wide, axis=-1, keepdims=True) + 1e-06)
            normed[to, :] = (wide * scale * gain_ref[...]).astype(BF16)

    def by_size(body):
        pl.when(has_mid)(lambda: body(most + MID))
        pl.when(jnp.logical_not(has_mid))(lambda: body(most))

    def add_dot(u, blk, first=False, last=False):
        def piece(size):
            to = pl.ds(0, size)

            @pl.loop(0, 4)
            def _(i):
                at = pl.ds(pl.multiple_of(i * half_t, half_t), half_t)
                left = normed[at, pl.ds(pl.multiple_of(blk * depth, depth), depth)]
                value = jnp.dot(left, bw[u, blk, :, pl.ds(first_unit, size)], preferred_element_type=F32)
                if first:
                    acc[u, at, to] = value
                elif last:
                    hidden[at, to] = (acc[0, at, to] * (acc[1, at, to] + value)).astype(BF16)
                else:
                    acc[u, at, to] = acc[u, at, to] + value

        by_size(piece)

    def activate():
        def piece(size):
            to = pl.ds(0, size)

            @pl.loop(0, 2 * tokens // step)
            def _(i):
                at = pl.ds(pl.multiple_of(i * step, step), step)
                value = acc[0, at, to]
                acc[0, at, to] = value / (1.0 + jnp.exp(-value))

        by_size(piece)

    def place(blk, span, start, size):
        return (
            pl.ds(pl.multiple_of(start, size), size),
            pl.ds(pl.multiple_of(blk * cols + span[0], 128), span[1]),
        )

    def remote(src, dst, sems, at, to):
        return pltpu.make_async_remote_copy(
            src, dst, sems[0].at[at], sems[1].at[at], device_id=to, device_id_type=MESH)

    def to_mate(blk, i, span):
        return remote(part.at[blk, 1, :, :, :, pl.ds(*span)], r1.at[blk, :, :, :, pl.ds(*span)], (psend, precv), (blk, i), mate)

    def line_all(blk, i, span):
        return remote(sbuf.at[blk, 1, :, :, pl.ds(*span)], rz.at[blk, :, :, pl.ds(*span)], (wsend, wrecv), (blk, i), pair)

    def line_one(blk, i, span):
        return remote(sx.at[blk, 1, :, pl.ds(*span)], rz.at[blk, 0, :, pl.ds(*span)], (wsend, wrecv), (blk, i), pair)

    def cross_all(blk, i, span):
        return remote(sx.at[blk, :, :, pl.ds(*span)], r2.at[blk, :, :, pl.ds(*span)], (xsend, xrecv), (blk, i), across)

    def cross_one(blk, i, span):
        return remote(sbuf.at[blk, :, 1 - row, :, pl.ds(*span)], r2.at[blk, :, :, pl.ds(*span)], (xsend, xrecv), (blk, i), across)

    def share(blk, i, span, who):
        at = outv.at[place(blk, span, c * half_t + who * quarter, quarter)]
        return remote(at, at, (asend, arecv), (blk, i), across)

    def give(blk, i, span, who):
        at = outv.at[place(blk, span, who * half_t, half_t)]
        return remote(at, at, (qsend, qrecv), (blk, i), mate)

    def write(blk, i, span):
        at = pl.ds(pl.multiple_of(blk * cols + span[0], 128), span[1])
        return pltpu.make_async_copy(outv.at[:, at], out_ref.at[:, at], osem.at[blk, i])

    def make_part(blk, i, span):
        def fill(size, side):
            @pl.loop(0, 2)
            def _(which):
                whose = c + side - 2 * c * side
                at = pl.ds(pl.multiple_of(which * tokens + whose * half_t, half_t), half_t)
                value = jnp.dot(
                    hidden[at, pl.ds(0, size)], bd[blk, pl.ds(first_unit, size), pl.ds(*span)],
                    preferred_element_type=F32)
                part[blk, side, which, :, :, pl.ds(*span)] = value.astype(BF16).reshape(2, quarter, span[1])

        by_size(lambda size: fill(size, 1))
        to_mate(blk, i, span).start()
        by_size(lambda size: fill(size, 0))

    def sum_mate(blk, i, span):
        to_mate(blk, i, span).wait_recv()
        at = pl.ds(*span)
        sbuf[blk, :, :, :, at] = (part[blk, 0, :, :, :, at].astype(F32) + r1[blk, :, :, :, at].astype(F32)).astype(BF16)

    def direct_1(blk, i, span):
        sum_mate(blk, i, span)
        line_all(blk, i, span).start()

    def direct_2(blk, i, span):
        line_all(blk, i, span).wait_recv()
        at = pl.ds(*span)
        sx[blk, :, :, at] = (sbuf[blk, 0, :, :, at].astype(F32) + rz[blk, :, :, at].astype(F32)).astype(BF16)
        cross_all(blk, i, span).start()

    def direct_3(blk, i, span):
        cross_all(blk, i, span).wait_recv()
        at = pl.ds(*span)
        value = (sx[blk, :, :, at].astype(F32) + r2[blk, :, :, at].astype(F32)).astype(BF16)
        outv[place(blk, span, c * half_t, half_t)] = value.reshape(half_t, span[1])
        give(blk, i, span, c).start()

    def split_1(blk, i, span):
        sum_mate(blk, i, span)
        cross_one(blk, i, span).start()

    def split_2(blk, i, span):
        cross_one(blk, i, span).wait_recv()
        at = pl.ds(*span)
        sx[blk, :, :, at] = (sbuf[blk, :, row, :, at].astype(F32) + r2[blk, :, :, at].astype(F32)).astype(BF16)
        line_one(blk, i, span).start()

    def split_3(blk, i, span):
        line_one(blk, i, span).wait_recv()
        at = pl.ds(*span)
        outv[place(blk, span, c * half_t + row * quarter, quarter)] = (
            sx[blk, 0, :, at].astype(F32) + rz[blk, 0, :, at].astype(F32)).astype(BF16)
        share(blk, i, span, row).start()

    def split_4(blk, i, span):
        share(blk, i, span, 1 - row).wait_recv()
        give(blk, i, span, c).start()

    def store(blk, i, span):
        give(blk, i, span, 1 - c).wait_recv()
        write(blk, i, span).start()

    stages = ((split_1, split_2, split_3, split_4, store), (direct_1, direct_2, direct_3, store))

    def way_of(blk):
        return jnp.where(blk < z, ONE, ZERO)

    def arrive(u, blk, rs=(0, 1, 2)):
        way = way_of(blk)
        for r in rs:
            @pl.when(arrives(r, way))
            def _():
                for s in pieces(r):
                    along(u, blk, r, s, way).wait_recv()
                    pl.when(passes(r, way))(lambda: along(u, blk, r, s, way).start())
                    pl.when(side_of(r, way) == e)(lambda: swap(u, blk, int(r == 1), s, y).start())

    def swaps(u, blk, who, body):
        for s in pieces(0):
            body(swap(u, blk, 0, s, who))

        @pl.when(has_mid)
        def _():
            for s in pieces(1):
                body(swap(u, blk, 1, s, who))

    def d_arrive(blk, i, span, rs=(0, 1, 2)):
        way = way_of(blk)
        for r in rs:
            @pl.when(arrives(r, way))
            def _():
                d_along(blk, i, span, r, way).wait_recv()
                pl.when(passes(r, way))(lambda: d_along(blk, i, span, r, way).start())
                pl.when(side_of(r, way) == e)(lambda: d_swap(blk, i, span, int(r == 1), y).start())

    def d_swaps(blk, i, span, who, body):
        body(d_swap(blk, i, span, 0, who))
        pl.when(has_mid)(lambda: body(d_swap(blk, i, span, 1, who)))

    def use(u, blk, last=False):
        swaps(u, blk, 1 - y, lambda copy: copy.wait_recv())
        add_dot(u, blk, last=last)

    zero_in = jnp.where(inner, ZERO, ONE)
    events = (
        (ZERO, jnp.where(inner, third, near)),
        (zero_in, near),
        (1 - zero_in, third),
        (ONE, jnp.where(inner, near, third)),
        (ZERO, fourth),
        (ONE, fourth),
    )

    tok_copy.wait()
    norm(tokv, 0)
    for copy in locals_:
        copy.wait()
    token_move(t, pair, 0, True).wait_recv()
    for i, one in enumerate(others):
        token_move(t, one, 1 + i, False).start()
    outer = jnp.logical_not(inner)
    arrive(*events[0])
    arrive(*events[1])
    arrive(*events[2])
    for d in (1, 2, 3):
        token_move(lax.rem(t + d, 4), mate, 0, False).wait_recv()
    norm(tokp, tokens)
    pl.when(inner)(lambda: arrive(*events[3], rs=(0,)))
    for u in (0, 1):
        add_dot(u, z, first=True)
    pl.when(inner)(lambda: arrive(*events[4], rs=(0, 1)))
    pl.when(outer)(lambda: arrive(*events[3]))
    use(*events[0])

    @pl.when(inner)
    def _():
        arrive(*events[3], rs=(1, 2))
        own_d_pieces(0, inward, go)

    use(*events[1])
    use(*events[2])
    pl.when(inner)(lambda: arrive(*events[4], rs=(2,)))
    pl.when(outer)(lambda: arrive(*events[4]))
    use(*events[3])

    @pl.when(inner)
    def _():
        d_arrive(first_block, 0, spans[1][0])
        arrive(*events[5], rs=(0,))

    use(*events[4])

    @pl.when(inner)
    def _():
        arrive(*events[5], rs=(1,))
        own_d_pieces(0, outward, go)

    activate()
    pl.when(outer)(lambda: arrive(*events[5]))

    @pl.when(inner)
    def _():
        arrive(*events[5], rs=(2,))
        for i in range(1, len(spans[1])):
            d_arrive(first_block, i, spans[1][i])
    blocks = (first_block, second_block, third, fourth)
    for kind, s, i in plan(cols):
        blk, span = blocks[s], spans[KINDS[s]][i]
        if kind == "last":
            use(*events[5], last=True)
        elif kind == "far":
            pl.when(inner)(lambda: d_arrive(blk, i, span, (0, 1)))
        elif kind == "near":
            pl.when(inner)(lambda: d_arrive(blk, i, span, (2,)))
        elif kind == "end":
            pl.when(outer)(lambda: d_arrive(blk, i, span))
        elif kind == "use":
            if s < 2:
                pl.when(blk != z)(lambda: d_swaps(blk, i, span, 1 - y, lambda copy: copy.wait_recv()))
            else:
                d_swaps(blk, i, span, 1 - y, lambda copy: copy.wait_recv())
            make_part(blk, i, span)
        else:
            stages[direct(s, i)][kind - 1](blk, i, span)

    token_move(t, pair, 0, True).wait_send()
    for i, one in enumerate(others):
        token_move(t, one, 1 + i, False).wait_send()
    sent = lambda copy: copy.wait_send()
    own_pieces(inward, sent)

    @pl.when(inner)
    def _():
        own_pieces(outward, sent)
        own_d_pieces(0, inward, sent)
        own_d_pieces(0, outward, sent)

    pl.when(jnp.logical_not(inner))(lambda: own_d_pieces(1, inward, sent))

    for s, blk in enumerate(blocks):
        def settle():
            way = way_of(blk)
            for r in range(3):
                @pl.when(jnp.logical_and(arrives(r, way), passes(r, way)))
                def _():
                    for u in (0, 1):
                        for piece in pieces(r):
                            along(u, blk, r, piece, way).wait_send()
                    for i, span in enumerate(spans[KINDS[s]]):
                        d_along(blk, i, span, r, way).wait_send()

            for u in (0, 1):
                swaps(u, blk, y, sent)
            for i, span in enumerate(spans[KINDS[s]]):
                d_swaps(blk, i, span, y, sent)

        pl.when(blk != z)(settle)
        for i, span in enumerate(spans[KINDS[s]]):
            to_mate(blk, i, span).wait_send()
            if direct(s, i):
                line_all(blk, i, span).wait_send()
                cross_all(blk, i, span).wait_send()
            else:
                cross_one(blk, i, span).wait_send()
                line_one(blk, i, span).wait_send()
                share(blk, i, span, row).wait_send()
            give(blk, i, span, c).wait_send()
            write(blk, i, span).wait()


def fused(n, tokens, norm_gain, gate_weight, up_weight, down_weight):
    rows, width = tokens.shape
    depth, units = gate_weight.shape
    cols = down_weight.shape[1]
    held = (units + MID) // 2
    dma = pltpu.SemaphoreType.DMA
    grid_of = (n, MOST_CUTS)
    quarter = rows // 4
    hbm = pl.BlockSpec(memory_space=pl.ANY)
    vmem = pl.BlockSpec(memory_space=pltpu.VMEM)
    return pl.pallas_call(
        functools.partial(kernel, n),
        out_shape=jax.ShapeDtypeStruct((rows, width), BF16),
        in_specs=[hbm, vmem, hbm, hbm, hbm],
        out_specs=hbm,
        scratch_shapes=[
            pltpu.VMEM((rows, width), BF16),
            pltpu.VMEM((rows, width), BF16),
            pltpu.VMEM((2 * rows, width), BF16),
            pltpu.VMEM((2, n, depth, units), BF16),
            pltpu.VMEM((n, units, cols), BF16),
            pltpu.VMEM((2, 2 * rows, held), F32),
            pltpu.VMEM((2 * rows, held), BF16),
            pltpu.VMEM((n, 2, 2, 2, quarter, cols), BF16),
            pltpu.VMEM((n, 2, 2, quarter, cols), BF16),
            pltpu.VMEM((n, 2, 2, quarter, cols), BF16),
            pltpu.VMEM((n, 2, quarter, cols), BF16),
            pltpu.VMEM((n, 2, quarter, cols), BF16),
            pltpu.VMEM((n, 2, quarter, cols), BF16),
            pltpu.VMEM((rows, width), BF16),
            dma((4,)),
            dma((2, n, 3, SUBS, 2)),
            dma((2, n, 3, SUBS)),
            dma((n, MOST_CUTS, 3, 2)),
            dma((n, MOST_CUTS, 3)),
            dma((2, n, 2, SUBS)),
            dma((2, n, 2, SUBS)),
            dma((n, MOST_CUTS, 2)),
            dma((n, MOST_CUTS, 2)),
            dma((4,)),
            dma((4,)),
        ] + [dma(grid_of) for _ in range(11)],
        compiler_params=pltpu.CompilerParams(
            collective_id=0, has_side_effects=True, vmem_limit_bytes=60 * 2**20
        ),
    )(tokens, norm_gain.reshape(1, width), gate_weight, up_weight, down_weight)


def solution(mesh):
    n = mesh.shape["fs"]
    small = mesh.shape["rep"] == 2 and mesh.shape["tp"] == 4 and n == 4
    body = functools.partial(fused, n) if small else plain
    in_specs = (P(("rep", "fs"), None), P(), P("fs", "tp"), P("fs", "tp"), P("tp", "fs"))
    out_specs = P(("rep", "fs"), None)
    return jax.shard_map(
        body, mesh=mesh, in_specs=in_specs, out_specs=out_specs, check_vma=False
    )
```

time: 147 us -> 131 us (0.89)
  Pallas kernels: 144 us -> 127 us
    pallas_call x1, Pallas kernels: 144 us -> 127 us  [fused(): pl.pallas_call(functools.partial(kernel, n), out_shape=jax.ShapeDtypeStru...]
where the time goes in v1:
time: 131 us
  Pallas kernels  127 us (97%)
  local copies, waits for them, and re-layouts  3.16 us (2%)
    pallas_call x1, Pallas kernels, fused(): pl.pallas_call(functools.partial(kernel, n), out_shape=jax.ShapeDtypeStru...  127 us
    unnamed x1, local copies, waits for them, and re-layouts  3.16 us

profile of v1, /device:TPU:1, one launch (start us, length us, event | category | flops | bytes accessed | tf_op | source)
XLA Modules:
  0.0 130.6 jit_solution(9213474313841317353)
XLA Ops:
  0.0 127.4 %shard_map.55 = bf16[512,2048]{1,0:T(8,128)(2,1)} custom-call(bf16[512,2048]{1,0:T(8,128)(2,1)} %tok_ref.1, f32[1,2048]{1,0:T(1,128)} %bitcast.1, bf16[512,1408]{1,0:T(8,128)(2,1)} %wg_ref.1, bf16[512,1408]{1,0:T(8,128)(2,1)} %wu_ref.1, bf16[1408,512]{1,0:T(8,128)(2,1)} %wd_ref.1), custom_call_target="tpu_custom_call" | custom-call | tf_op jit(solution)/shard_map/pallas_call | solution.py:584
  127.5 3.2 %copy.7 = bf16[512,2048]{1,0:T(8,128)(2,1)} copy(bf16[512,2048]{1,0:T(8,128)(2,1)} %shard_map.55) | data formatting | bytes 4194304

commit v2 on v1

--- a/solution.py
+++ b/solution.py
@@ -26,8 +26,10 @@
 
 CUTS = ((2, 2), (2, 1, 1))
 KINDS = (1, 0, 0, 1)
+DIRECT = (0, 1, 0, 1)
 MOST_CUTS = 3
 SUBS = 2
+SLACK = 0.0
 MID = 128
 
 
@@ -72,10 +74,10 @@
         todo.append((when, stage, s, i))
         size = spans_of(KINDS[s], width)[i][1]
         half = block * size / width * 5.5 / 15.4
-        path = ROUTES[direct(s, i)]
+        path = ROUTES[direct(s)]
         if stage <= len(path):
             link, scale = path[stage - 1]
-            after = when + 1.5 if link == "core" else book(link, when, half * scale) + hop
+            after = when + 1.5 if link == "core" else book(link, when, half * scale) + hop + SLACK
             pend.append((after, stage + 1, s, i))
     todo.sort(key=lambda item: item[0])
     return [item[1:] for item in todo]
@@ -87,8 +89,8 @@
 )
 
 
-def direct(s, i):
-    return int(s == 3 or s == 1)
+def direct(s):
+    return DIRECT[s]
 
 
 def kernel(
@@ -115,7 +117,7 @@
     third = 2 - hi
     fourth = 3 - 3 * hi
     pair = {"fs": near}
-    has_mid = e == c
+    has_mid = inner
     mine = pl.multiple_of(e * (most + MID), MID)
     first_unit = pl.multiple_of(e * jnp.where(has_mid, most, most + MID), MID)
     mate = {"tp": t + 1 - 2 * c}
@@ -152,7 +154,10 @@
         return pl.multiple_of(side * (most + MID), MID), most
 
     def side_of(r, way):
-        return c if r == 1 else (way if r == 0 else 1 - way)
+        return way if r == 0 else 1 - way
+
+    def kept(r, way):
+        return inner if r == 1 else side_of(r, way) == e
 
     def passes(r, way):
         q = side_of(r, way)
@@ -178,8 +183,8 @@
         return pltpu.make_async_remote_copy(
             src_ref=bw.at[(u, blk) + at] if own is None else own.at[at],
             dst_ref=bw.at[(u, blk) + at],
-            send_sem=zsend.at[u, blk, r, s, way],
-            recv_sem=zrecv.at[u, blk, r, s],
+            send_sem=zsend.at[blk, way],
+            recv_sem=zrecv.at[u, blk, (0, SUBS, SUBS + 1)[r] + s],
             device_id={"fs": z - 1 + 2 * way},
             device_id_type=MESH,
         )
@@ -190,8 +195,8 @@
         return pltpu.make_async_remote_copy(
             src_ref=place,
             dst_ref=place,
-            send_sem=ysend.at[u, blk, i, s],
-            recv_sem=yrecv.at[u, blk, i, s],
+            send_sem=ysend.at[blk],
+            recv_sem=yrecv.at[u, blk],
             device_id=peer,
             device_id_type=MESH,
         )
@@ -205,7 +210,7 @@
         return pltpu.make_async_remote_copy(
             src_ref=wd_ref.at[at] if own else bd.at[(blk,) + at],
             dst_ref=bd.at[(blk,) + at],
-            send_sem=dsend.at[blk, i, r, way],
+            send_sem=dsend.at[blk, way],
             recv_sem=drecv.at[blk, i, r],
             device_id={"fs": z - 1 + 2 * way},
             device_id_type=MESH,
@@ -217,8 +222,8 @@
         return pltpu.make_async_remote_copy(
             src_ref=place,
             dst_ref=place,
-            send_sem=vsend.at[blk, i, p],
-            recv_sem=vrecv.at[blk, i, p],
+            send_sem=vsend.at[blk],
+            recv_sem=vrecv.at[blk, i],
             device_id=peer,
             device_id_type=MESH,
         )
@@ -274,15 +279,18 @@
         pl.when(has_mid)(lambda: body(most + MID))
         pl.when(jnp.logical_not(has_mid))(lambda: body(most))
 
-    def add_dot(u, blk, first=False, last=False):
+    def add_dot(u, blk, first=False, last=False, start=0, rows=None):
+        rows = depth if rows is None else rows
+
         def piece(size):
             to = pl.ds(0, size)
 
             @pl.loop(0, 4)
             def _(i):
                 at = pl.ds(pl.multiple_of(i * half_t, half_t), half_t)
-                left = normed[at, pl.ds(pl.multiple_of(blk * depth, depth), depth)]
-                value = jnp.dot(left, bw[u, blk, :, pl.ds(first_unit, size)], preferred_element_type=F32)
+                left = normed[at, pl.ds(pl.multiple_of(blk * depth + start, rows), rows)]
+                right = bw[u, blk, pl.ds(pl.multiple_of(start, rows), rows), pl.ds(first_unit, size)]
+                value = jnp.dot(left, right, preferred_element_type=F32)
                 if first:
                     acc[u, at, to] = value
                 elif last:
@@ -312,7 +320,7 @@
 
     def remote(src, dst, sems, at, to):
         return pltpu.make_async_remote_copy(
-            src, dst, sems[0].at[at], sems[1].at[at], device_id=to, device_id_type=MESH)
+            src, dst, sems[0].at[at[0]], sems[1].at[at], device_id=to, device_id_type=MESH)
 
     def to_mate(blk, i, span):
         return remote(part.at[blk, 1, :, :, :, pl.ds(*span)], r1.at[blk, :, :, :, pl.ds(*span)], (psend, precv), (blk, i), mate)
@@ -339,7 +347,7 @@
 
     def write(blk, i, span):
         at = pl.ds(pl.multiple_of(blk * cols + span[0], 128), span[1])
-        return pltpu.make_async_copy(outv.at[:, at], out_ref.at[:, at], osem.at[blk, i])
+        return pltpu.make_async_copy(outv.at[:, at], out_ref.at[:, at], osem.at[blk])
 
     def make_part(blk, i, span):
         def fill(size, side):
@@ -416,16 +424,17 @@
                 for s in pieces(r):
                     along(u, blk, r, s, way).wait_recv()
                     pl.when(passes(r, way))(lambda: along(u, blk, r, s, way).start())
-                    pl.when(side_of(r, way) == e)(lambda: swap(u, blk, int(r == 1), s, y).start())
-
-    def swaps(u, blk, who, body):
-        for s in pieces(0):
-            body(swap(u, blk, 0, s, who))
-
-        @pl.when(has_mid)
-        def _():
-            for s in pieces(1):
-                body(swap(u, blk, 1, s, who))
+                    pl.when(kept(r, way))(lambda: swap(u, blk, int(r == 1), s, y).start())
+
+    def all_received(ref, sem):
+        pltpu.make_async_remote_copy(ref, ref, zsend.at[0, 0], sem, device_id=peer, device_id_type=MESH).wait_recv()
+
+    def all_sent(ref, sem):
+        pltpu.make_async_remote_copy(ref, ref, sem, zrecv.at[0, 0, 0], device_id=peer, device_id_type=MESH).wait_send()
+
+    def swapped(u, blk):
+        rows = pl.ds(pl.multiple_of((1 - y) * half_k, half_k), half_k)
+        by_size(lambda size: all_received(bw.at[u, blk, rows, pl.ds(first_unit, size)], yrecv.at[u, blk]))
 
     def d_arrive(blk, i, span, rs=(0, 1, 2)):
         way = way_of(blk)
@@ -434,15 +443,19 @@
             def _():
                 d_along(blk, i, span, r, way).wait_recv()
                 pl.when(passes(r, way))(lambda: d_along(blk, i, span, r, way).start())
-                pl.when(side_of(r, way) == e)(lambda: d_swap(blk, i, span, int(r == 1), y).start())
-
-    def d_swaps(blk, i, span, who, body):
-        body(d_swap(blk, i, span, 0, who))
-        pl.when(has_mid)(lambda: body(d_swap(blk, i, span, 1, who)))
+                pl.when(kept(r, way))(lambda: d_swap(blk, i, span, int(r == 1), y).start())
+
+    def d_swapped(blk, i, span):
+        by_size(lambda size: all_received(bd.at[blk, pl.ds(0, size // 2), pl.ds(*span)], vrecv.at[blk, i]))
 
     def use(u, blk, last=False):
-        swaps(u, blk, 1 - y, lambda copy: copy.wait_recv())
-        add_dot(u, blk, last=last)
+        if last:
+            add_dot(u, blk, start=y * half_k, rows=half_k)
+            swapped(u, blk)
+            add_dot(u, blk, last=True, start=(1 - y) * half_k, rows=half_k)
+        else:
+            swapped(u, blk)
+            add_dot(u, blk)
 
     zero_in = jnp.where(inner, ZERO, ONE)
     events = (
@@ -519,56 +532,53 @@
             pl.when(outer)(lambda: d_arrive(blk, i, span))
         elif kind == "use":
             if s < 2:
-                pl.when(blk != z)(lambda: d_swaps(blk, i, span, 1 - y, lambda copy: copy.wait_recv()))
+                pl.when(blk != z)(lambda: d_swapped(blk, i, span))
             else:
-                d_swaps(blk, i, span, 1 - y, lambda copy: copy.wait_recv())
+                d_swapped(blk, i, span)
             make_part(blk, i, span)
         else:
-            stages[direct(s, i)][kind - 1](blk, i, span)
+            stages[direct(s)][kind - 1](blk, i, span)
 
     token_move(t, pair, 0, True).wait_send()
     for i, one in enumerate(others):
         token_move(t, one, 1 + i, False).wait_send()
-    sent = lambda copy: copy.wait_send()
-    own_pieces(inward, sent)
-
-    @pl.when(inner)
-    def _():
-        own_pieces(outward, sent)
-        own_d_pieces(0, inward, sent)
-        own_d_pieces(0, outward, sent)
-
-    pl.when(jnp.logical_not(inner))(lambda: own_d_pieces(1, inward, sent))
-
+
+    def sent_along(blk, way):
+        def wait(size):
+            all_sent(bw.at[:, blk, pl.ds(0, half_k), pl.ds(0, size)], zsend.at[blk, way])
+            all_sent(bd.at[blk, pl.ds(0, size // 2)], dsend.at[blk, way])
+
+        some = jnp.logical_and(passes(0, way), jnp.logical_not(passes(2, way)))
+        pl.when(passes(2, way))(lambda: wait(units))
+        pl.when(jnp.logical_and(some, passes(1, way)))(lambda: wait(most + MID))
+        pl.when(jnp.logical_and(some, jnp.logical_not(passes(1, way))))(lambda: wait(most))
+
+    def sent_swap(blk):
+        def wait(size):
+            all_sent(bw.at[:, blk, pl.ds(0, half_k), pl.ds(0, size)], ysend.at[blk])
+            all_sent(bd.at[blk, pl.ds(0, size // 2)], vsend.at[blk])
+
+        by_size(wait)
+
+    sent_along(z, ZERO)
+    sent_along(z, ONE)
+    whole = (0, cols)
     for s, blk in enumerate(blocks):
         def settle():
-            way = way_of(blk)
-            for r in range(3):
-                @pl.when(jnp.logical_and(arrives(r, way), passes(r, way)))
-                def _():
-                    for u in (0, 1):
-                        for piece in pieces(r):
-                            along(u, blk, r, piece, way).wait_send()
-                    for i, span in enumerate(spans[KINDS[s]]):
-                        d_along(blk, i, span, r, way).wait_send()
-
-            for u in (0, 1):
-                swaps(u, blk, y, sent)
-            for i, span in enumerate(spans[KINDS[s]]):
-                d_swaps(blk, i, span, y, sent)
+            sent_along(blk, way_of(blk))
+            sent_swap(blk)
 
         pl.when(blk != z)(settle)
-        for i, span in enumerate(spans[KINDS[s]]):
-            to_mate(blk, i, span).wait_send()
-            if direct(s, i):
-                line_all(blk, i, span).wait_send()
-                cross_all(blk, i, span).wait_send()
-            else:
-                cross_one(blk, i, span).wait_send()
-                line_one(blk, i, span).wait_send()
-                share(blk, i, span, row).wait_send()
-            give(blk, i, span, c).wait_send()
-            write(blk, i, span).wait()
+        all_sent(part.at[blk, 1], psend.at[blk])
+        if direct(s):
+            all_sent(sbuf.at[blk, 1], wsend.at[blk])
+            all_sent(sx.at[blk], xsend.at[blk])
+        else:
+            all_sent(sbuf.at[blk, :, 0], xsend.at[blk])
+            all_sent(sx.at[blk, 1], wsend.at[blk])
+            all_sent(outv.at[place(blk, whole, 0, quarter)], asend.at[blk])
+        all_sent(outv.at[place(blk, whole, 0, half_t)], qsend.at[blk])
+        write(blk, 0, whole).wait()
 
 
 def fused(n, tokens, norm_gain, gate_weight, up_weight, down_weight):
@@ -577,7 +587,6 @@
     cols = down_weight.shape[1]
     held = (units + MID) // 2
     dma = pltpu.SemaphoreType.DMA
-    grid_of = (n, MOST_CUTS)
     quarter = rows // 4
     hbm = pl.BlockSpec(memory_space=pl.ANY)
     vmem = pl.BlockSpec(memory_space=pltpu.VMEM)
@@ -602,17 +611,17 @@
             pltpu.VMEM((n, 2, quarter, cols), BF16),
             pltpu.VMEM((rows, width), BF16),
             dma((4,)),
-            dma((2, n, 3, SUBS, 2)),
-            dma((2, n, 3, SUBS)),
-            dma((n, MOST_CUTS, 3, 2)),
+            dma((n, 2)),
+            dma((2, n, 2 * SUBS + 1)),
+            dma((n, 2)),
             dma((n, MOST_CUTS, 3)),
-            dma((2, n, 2, SUBS)),
-            dma((2, n, 2, SUBS)),
-            dma((n, MOST_CUTS, 2)),
-            dma((n, MOST_CUTS, 2)),
+            dma((n,)),
+            dma((2, n)),
+            dma((n,)),
+            dma((n, MOST_CUTS)),
             dma((4,)),
             dma((4,)),
-        ] + [dma(grid_of) for _ in range(11)],
+        ] + 5 * [dma((n,)), dma((n, MOST_CUTS))] + [dma((n,))],
         compiler_params=pltpu.CompilerParams(
             collective_id=0, has_side_effects=True, vmem_limit_bytes=60 * 2**20
         ),

time: 131 us -> 128 us (0.977)
  Pallas kernels: 127 us -> 124 us
    pallas_call x1, Pallas kernels: 127 us -> 124 us  [fused(): pl.pallas_call(functools.partial(kernel, n), out_shape=jax.ShapeDtypeStru...]
where the time goes in v2:
time: 128 us; the launch traced here: 127 us
  Pallas kernels  124 us (97%)
  local copies, waits for them, and re-layouts  3.16 us (2%)
    pallas_call x1, Pallas kernels, fused(): pl.pallas_call(functools.partial(kernel, n), out_shape=jax.ShapeDtypeStru...  124 us
    unnamed x1, local copies, waits for them, and re-layouts  3.16 us

profile of v2, /device:TPU:1, one launch (start us, length us, event | category | flops | bytes accessed | tf_op | source)
XLA Modules:
  0.0 127.3 jit_solution(4684394000618699415)
XLA Ops:
  0.0 124.2 %shard_map.55 = bf16[512,2048]{1,0:T(8,128)(2,1)} custom-call(bf16[512,2048]{1,0:T(8,128)(2,1)} %tok_ref.1, f32[1,2048]{1,0:T(1,128)} %bitcast.1, bf16[512,1408]{1,0:T(8,128)(2,1)} %wg_ref.1, bf16[512,1408]{1,0:T(8,128)(2,1)} %wu_ref.1, bf16[1408,512]{1,0:T(8,128)(2,1)} %wd_ref.1), custom_call_target="tpu_custom_call" | custom-call | tf_op jit(solution)/shard_map/pallas_call | solution.py:593
  124.2 3.2 %copy.7 = bf16[512,2048]{1,0:T(8,128)(2,1)} copy(bf16[512,2048]{1,0:T(8,128)(2,1)} %shard_map.55) | data formatting | bytes 4194304

commit v3 on v2

--- a/solution.py
+++ b/solution.py
@@ -24,68 +24,37 @@
     return lax.psum(partial_value.astype(BF16), "tp")
 
 
-CUTS = ((2, 2), (2, 1, 1))
-KINDS = (1, 0, 0, 1)
-DIRECT = (0, 1, 0, 1)
-MOST_CUTS = 3
+CUTS = (1, 1, 1, 1)
+DIRECT = (0, 0, 0, 1)
+MOST_CUTS = 4
 SUBS = 2
-SLACK = 0.0
 MID = 128
 
 
-def spans_of(which, width):
+def spans_of(width):
     spans, at = [], 0
-    for part in CUTS[which]:
+    for part in CUTS:
         spans.append((at, part * width // 4))
         at += part * width // 4
     return spans
 
 
-def plan(width):
-    block, hop, start = 15.4, 2.2, 67.2
-    free = {"x": 0.0, "z": 0.0, "weights": 71.7, "core": 74.0}
-    todo = [(72.0, "last", 0, 0)]
-
-    def book(link, when, size):
-        free[link] = max(free[link], when) + size
-        return free[link]
-
-    for s in range(4):
-        for i, (at, size) in enumerate(spans_of(KINDS[s], width)):
-            share = block * size / width
-            ready = 70.0
-            if s == 1:
-                out = 64.0 + block * (at + size) / width / 2 + hop
-                todo.append((out, "end", s, i))
-                ready = out + share / 2 + hop
-            if s >= 2:
-                begin = start + (s - 2) * block + block * at / width
-                far, near = begin + 0.55 * share + hop, begin + share + hop
-                out = book("weights", far, share / 2) + hop
-                todo += [(far, "far", s, i), (near, "near", s, i), (out, "end", s, i)]
-                ready = max(near, out) + share / 2 + hop
-            done = book("core", ready, 1.2 * size / 256 + 0.2)
-            todo.append((done, "use", s, i))
-    uses = [(when, s, i) for when, kind, s, i in todo if kind == "use"]
-    pend = [(when + 1.8, 1, s, i) for when, s, i in uses]
-    while pend:
-        pend.sort()
-        when, stage, s, i = pend.pop(0)
-        todo.append((when, stage, s, i))
-        size = spans_of(KINDS[s], width)[i][1]
-        half = block * size / width * 5.5 / 15.4
-        path = ROUTES[direct(s)]
-        if stage <= len(path):
-            link, scale = path[stage - 1]
-            after = when + 1.5 if link == "core" else book(link, when, half * scale) + hop + SLACK
-            pend.append((after, stage + 1, s, i))
-    todo.sort(key=lambda item: item[0])
-    return [item[1:] for item in todo]
-
-
-ROUTES = (
-    (("x", 1.0), ("z", 0.8), ("x", 0.5), ("core", 0.0)),
-    (("z", 1.0), ("x", 1.0), ("core", 0.0)),
+ORDER = (
+    ("end", 1, 0), ("last", 0, 0), ("far", 2, 0), ("far", 2, 1), ("near", 2, 0), ("end", 1, 1), ("use", 0, 1),
+    ("use", 0, 3), (1, 0, 1), ("use", 1, 0), (1, 1, 0), (1, 0, 3), ("end", 1, 2), ("far", 2, 2),
+    ("use", 1, 1), ("near", 2, 1), ("end", 1, 3), ("end", 2, 0), ("use", 0, 0), ("near", 2, 2), ("use", 0, 2),
+    (2, 1, 0), (1, 0, 0), ("far", 2, 3), (1, 0, 2), (2, 0, 1), ("end", 2, 1), ("use", 1, 3), ("use", 1, 2),
+    ("far", 3, 0), ("near", 2, 3), (2, 0, 3), (1, 1, 1), ("use", 2, 0), ("end", 2, 2), (2, 0, 0),
+    ("near", 3, 0), (1, 1, 3), ("use", 2, 1), (1, 2, 0), ("far", 3, 1), (2, 0, 2), (1, 1, 2), ("end", 2, 3),
+    (2, 1, 1), ("end", 3, 0), (3, 0, 0), ("use", 2, 2), ("near", 3, 1), (2, 1, 3), ("far", 3, 2), (1, 2, 1),
+    (2, 1, 2), (2, 2, 0), ("end", 3, 1), (1, 2, 2), ("use", 2, 3), (3, 0, 1), ("use", 3, 0), (1, 2, 3),
+    ("end", 3, 2), (4, 0, 0), ("far", 3, 3), ("near", 3, 2), (3, 1, 0), (1, 3, 0), ("use", 3, 1), (3, 0, 2),
+    (3, 0, 3), ("near", 3, 3), (3, 1, 2), (3, 1, 1), (1, 3, 1), (2, 2, 1), ("end", 3, 3), (3, 2, 0),
+    (5, 0, 0), (2, 2, 2), ("use", 3, 2), (2, 2, 3), (4, 0, 2), (4, 0, 1), (2, 3, 0), (2, 3, 1), (1, 3, 2),
+    (4, 1, 0), (3, 1, 3), (3, 2, 1), ("use", 3, 3), (4, 0, 3), (3, 2, 2), (1, 3, 3), (5, 0, 3), (3, 2, 3),
+    (5, 0, 1), (4, 1, 1), (2, 3, 2), (4, 2, 0), (2, 3, 3), (3, 3, 1), (3, 3, 0), (4, 1, 2), (4, 3, 0),
+    (4, 2, 3), (4, 1, 3), (4, 2, 2), (5, 1, 2), (3, 3, 2), (4, 3, 1), (5, 0, 2), (5, 2, 2), (5, 1, 0),
+    (5, 2, 3), (5, 2, 0), (5, 1, 1), (4, 2, 1), (3, 3, 3), (4, 3, 2), (5, 1, 3), (5, 2, 1), (4, 3, 3),
 )
 
 
@@ -106,7 +75,7 @@
     tokens, width = tok_ref.shape
     depth, units = wg_ref.shape
     cols = wd_ref.shape[1]
-    spans = tuple(spans_of(which, cols) for which in (0, 1))
+    spans = spans_of(cols)
     half_k, half_t, quarter = depth // 2, tokens // 2, tokens // 4
     sub_k = half_k // SUBS
     most = (units - MID) // 2
@@ -123,7 +92,6 @@
     mate = {"tp": t + 1 - 2 * c}
     across = {"tp": lax.rem(t + 2, 4)}
     row = t // 2
-    first_block, second_block = 3 * hi, 1 + hi
     peer = {"rep": 1 - y}
 
     barrier = pltpu.get_barrier_semaphore()
@@ -236,8 +204,8 @@
                     for s in pieces(r):
                         body(along(u, z, r, s, way, own))
 
-    def own_d_pieces(which, way, body):
-        for i, span in enumerate(spans[which]):
+    def own_d_pieces(way, body):
+        for i, span in enumerate(spans):
             for r in range(3):
                 pl.when(passes(r, way))(lambda: body(d_along(z, i, span, r, way, True)))
 
@@ -254,7 +222,7 @@
     def _():
         token_move(t, pair, 0, True).start()
         own_pieces(inward, go)
-        own_d_pieces(1, inward, go)
+        own_d_pieces(inward, go)
 
     locals_ = [
         pltpu.make_async_copy(wg_ref, bw.at[0, z], loc_sem.at[0]),
@@ -491,7 +459,7 @@
     @pl.when(inner)
     def _():
         arrive(*events[3], rs=(1, 2))
-        own_d_pieces(0, inward, go)
+        own_d_pieces(inward, go)
 
     use(*events[1])
     use(*events[2])
@@ -501,7 +469,6 @@
 
     @pl.when(inner)
     def _():
-        d_arrive(first_block, 0, spans[1][0])
         arrive(*events[5], rs=(0,))
 
     use(*events[4])
@@ -509,7 +476,7 @@
     @pl.when(inner)
     def _():
         arrive(*events[5], rs=(1,))
-        own_d_pieces(0, outward, go)
+        own_d_pieces(outward, go)
 
     activate()
     pl.when(outer)(lambda: arrive(*events[5]))
@@ -517,11 +484,11 @@
     @pl.when(inner)
     def _():
         arrive(*events[5], rs=(2,))
-        for i in range(1, len(spans[1])):
-            d_arrive(first_block, i, spans[1][i])
-    blocks = (first_block, second_block, third, fourth)
-    for kind, s, i in plan(cols):
-        blk, span = blocks[s], spans[KINDS[s]][i]
+        for i, span in enumerate(spans):
+            d_arrive(near, i, span)
+    blocks = (z, near, third, fourth)
+    for kind, s, i in ORDER:
+        blk, span = blocks[s], spans[i]
         if kind == "last":
             use(*events[5], last=True)
         elif kind == "far":
@@ -531,9 +498,7 @@
         elif kind == "end":
             pl.when(outer)(lambda: d_arrive(blk, i, span))
         elif kind == "use":
-            if s < 2:
-                pl.when(blk != z)(lambda: d_swapped(blk, i, span))
-            else:
+            if s > 0:
                 d_swapped(blk, i, span)
             make_part(blk, i, span)
         else:
@@ -568,7 +533,8 @@
             sent_along(blk, way_of(blk))
             sent_swap(blk)
 
-        pl.when(blk != z)(settle)
+        if s > 0:
+            settle()
         all_sent(part.at[blk, 1], psend.at[blk])
         if direct(s):
             all_sent(sbuf.at[blk, 1], wsend.at[blk])

time: 128 us -> 121 us (0.945)
  Pallas kernels: 124 us -> 118 us
    pallas_call x1, Pallas kernels: 124 us -> 118 us  [fused(): pl.pallas_call(functools.partial(kernel, n), out_shape=jax.ShapeDtypeStru...]
where the time goes in v3:
time: 121 us
  Pallas kernels  118 us (98%)
  local copies, waits for them, and re-layouts  3.16 us (3%)
    pallas_call x1, Pallas kernels, fused(): pl.pallas_call(functools.partial(kernel, n), out_shape=jax.ShapeDtypeStru...  118 us
    unnamed x1, local copies, waits for them, and re-layouts  3.16 us

profile of v3, /device:TPU:1, one launch (start us, length us, event | category | flops | bytes accessed | tf_op | source)
XLA Modules:
  0.0 120.8 jit_solution(7964569226527607375)
XLA Ops:
  0.0 117.6 %shard_map.55 = bf16[512,2048]{1,0:T(8,128)(2,1)} custom-call(bf16[512,2048]{1,0:T(8,128)(2,1)} %tok_ref.1, f32[1,2048]{1,0:T(1,128)} %bitcast.1, bf16[512,1408]{1,0:T(8,128)(2,1)} %wg_ref.1, bf16[512,1408]{1,0:T(8,128)(2,1)} %wu_ref.1, bf16[1408,512]{1,0:T(8,128)(2,1)} %wd_ref.1), custom_call_target="tpu_custom_call" | custom-call | tf_op jit(solution)/shard_map/pallas_call | solution.py:559
  117.6 3.2 %copy.7 = bf16[512,2048]{1,0:T(8,128)(2,1)} copy(bf16[512,2048]{1,0:T(8,128)(2,1)} %shard_map.55) | data formatting | bytes 4194304

commit v4 on v3

--- a/solution.py
+++ b/solution.py
@@ -439,11 +439,12 @@
     norm(tokv, 0)
     for copy in locals_:
         copy.wait()
+    pl.when(inner)(lambda: arrive(*events[0]))
     token_move(t, pair, 0, True).wait_recv()
     for i, one in enumerate(others):
         token_move(t, one, 1 + i, False).start()
     outer = jnp.logical_not(inner)
-    arrive(*events[0])
+    pl.when(outer)(lambda: arrive(*events[0]))
     arrive(*events[1])
     arrive(*events[2])
     for d in (1, 2, 3):
@@ -558,7 +559,7 @@
     vmem = pl.BlockSpec(memory_space=pltpu.VMEM)
     return pl.pallas_call(
         functools.partial(kernel, n),
-        out_shape=jax.ShapeDtypeStruct((rows, width), BF16),
+        out_shape=pltpu.VMEM((rows, width), BF16),
         in_specs=[hbm, vmem, hbm, hbm, hbm],
         out_specs=hbm,
         scratch_shapes=[

time: 121 us -> 119 us (0.983)
  local copies, waits for them, and re-layouts: 3.16 us -> 1.32 us
    unnamed x1, local copies, waits for them, and re-layouts: 3.16 us -> 1.32 us
where the time goes in v4:
time: 119 us; the launch traced here: 118 us
  Pallas kernels  117 us (98%)
  local copies, waits for them, and re-layouts  1.32 us (1%)
    pallas_call x1, Pallas kernels, fused(): pl.pallas_call(functools.partial(kernel, n), out_shape=pltpu.VMEM((rows,...  117 us

profile of v4, /device:TPU:1, one launch (start us, length us, event | category | flops | bytes accessed | tf_op | source)
XLA Modules:
  0.0 118.4 jit_solution(11285685170463979513)
XLA Ops:
  0.0 117.1 %shard_map.55 = bf16[512,2048]{1,0:T(8,128)(2,1)S(1)} custom-call(bf16[512,2048]{1,0:T(8,128)(2,1)} %tok_ref.1, f32[1,2048]{1,0:T(1,128)} %bitcast.1, bf16[512,1408]{1,0:T(8,128)(2,1)} %wg_ref.1, bf16[512,1408]{1,0:T(8,128)(2,1)} %wu_ref.1, bf16[1408,512]{1,0:T(8,128)(2,1)} %wd_ref.1), custom_call_target="tpu_custom_call" | custom-call | tf_op jit(solution)/shard_map/pallas_call | solution.py:560
  117.1 1.3 %copy.7 = bf16[512,2048]{1,0:T(8,128)(2,1)} copy(bf16[512,2048]{1,0:T(8,128)(2,1)S(1)} %shard_map.55) | data formatting | bytes 4194304

commit v5 on v4

--- a/solution.py
+++ b/solution.py
@@ -63,10 +63,10 @@
 
 
 def kernel(
-    n, tok_ref, gain_ref, wg_ref, wu_ref, wd_ref, out_ref,
-    tokv, tokp, normed, bw, bd, acc, hidden, part, r1, sbuf, rz, sx, r2, outv,
+    n, tok_ref, gain_ref, wg_ref, wu_ref, wd_ref, outv,
+    tokv, tokp, normed, bw, bd, acc, hidden, part, r1, sbuf, rz, sx, r2,
     loc_sem, zsend, zrecv, dsend, drecv, ysend, yrecv, vsend, vrecv, tsend, trecv,
-    psend, precv, wsend, wrecv, xsend, xrecv, asend, arecv, qsend, qrecv, osem,
+    psend, precv, wsend, wrecv, xsend, xrecv, asend, arecv, qsend, qrecv,
 ):
     z = lax.axis_index("fs")
     y = lax.axis_index("rep")
@@ -313,10 +313,6 @@
         at = outv.at[place(blk, span, who * half_t, half_t)]
         return remote(at, at, (qsend, qrecv), (blk, i), mate)
 
-    def write(blk, i, span):
-        at = pl.ds(pl.multiple_of(blk * cols + span[0], 128), span[1])
-        return pltpu.make_async_copy(outv.at[:, at], out_ref.at[:, at], osem.at[blk])
-
     def make_part(blk, i, span):
         def fill(size, side):
             @pl.loop(0, 2)
@@ -377,7 +373,6 @@
 
     def store(blk, i, span):
         give(blk, i, span, 1 - c).wait_recv()
-        write(blk, i, span).start()
 
     stages = ((split_1, split_2, split_3, split_4, store), (direct_1, direct_2, direct_3, store))
 
@@ -545,7 +540,6 @@
             all_sent(sx.at[blk, 1], wsend.at[blk])
             all_sent(outv.at[place(blk, whole, 0, quarter)], asend.at[blk])
         all_sent(outv.at[place(blk, whole, 0, half_t)], qsend.at[blk])
-        write(blk, 0, whole).wait()
 
 
 def fused(n, tokens, norm_gain, gate_weight, up_weight, down_weight):
@@ -561,7 +555,7 @@
         functools.partial(kernel, n),
         out_shape=pltpu.VMEM((rows, width), BF16),
         in_specs=[hbm, vmem, hbm, hbm, hbm],
-        out_specs=hbm,
+        out_specs=vmem,
         scratch_shapes=[
             pltpu.VMEM((rows, width), BF16),
             pltpu.VMEM((rows, width), BF16),
@@ -576,7 +570,6 @@
             pltpu.VMEM((n, 2, quarter, cols), BF16),
             pltpu.VMEM((n, 2, quarter, cols), BF16),
             pltpu.VMEM((n, 2, quarter, cols), BF16),
-            pltpu.VMEM((rows, width), BF16),
             dma((4,)),
             dma((n, 2)),
             dma((2, n, 2 * SUBS + 1)),
@@ -588,7 +581,7 @@
             dma((n, MOST_CUTS)),
             dma((4,)),
             dma((4,)),
-        ] + 5 * [dma((n,)), dma((n, MOST_CUTS))] + [dma((n,))],
+        ] + 5 * [dma((n,)), dma((n, MOST_CUTS))],
         compiler_params=pltpu.CompilerParams(
             collective_id=0, has_side_effects=True, vmem_limit_bytes=60 * 2**20
         ),

time: 119 us -> 119 us (level)
  no operation moved by 1% of the time
where the time goes in v5:
time: 119 us; the launch traced here: 118 us
  Pallas kernels  117 us (98%)
  local copies, waits for them, and re-layouts  1.32 us (1%)
    pallas_call x1, Pallas kernels, fused(): pl.pallas_call(functools.partial(kernel, n), out_shape=pltpu.VMEM((rows,...  117 us

profile of v5, /device:TPU:1, one launch (start us, length us, event | category | flops | bytes accessed | tf_op | source)
XLA Modules:
  0.0 118.3 jit_solution(3537072032194058424)
XLA Ops:
  0.0 117.0 %shard_map.55 = bf16[512,2048]{1,0:T(8,128)(2,1)S(1)} custom-call(bf16[512,2048]{1,0:T(8,128)(2,1)} %tok_ref.1, f32[1,2048]{1,0:T(1,128)} %bitcast.1, bf16[512,1408]{1,0:T(8,128)(2,1)} %wg_ref.1, bf16[512,1408]{1,0:T(8,128)(2,1)} %wu_ref.1, bf16[1408,512]{1,0:T(8,128)(2,1)} %wd_ref.1), custom_call_target="tpu_custom_call" | custom-call | tf_op jit(solution)/shard_map/pallas_call | solution.py:554
  117.0 1.3 %copy.7 = bf16[512,2048]{1,0:T(8,128)(2,1)} copy(bf16[512,2048]{1,0:T(8,128)(2,1)S(1)} %shard_map.55) | data formatting | bytes 4194304
